TPU v7x, 32 devices: a whole 2x2x4 slice. The times are simulated.
32 devices in a mesh: grp: 2 (over x), tp: 16 (over z, y, core).
Axes of the slice: x: 2, y: 2, z: 4, core: 2. Of those that a mesh axis runs over, the one named last changes fastest.
Arguments:
- stream_in: bfloat16 [64, 4, 4096], P('grp'), parts along dimension 0, may hold values from -6 to 6
- state_in: float32 [2, 64, 8, 256, 256], P(None, 'grp', None, 'tp'), parts along dimension 1, may hold values from -0.8 to 0.8
- norm_gain: bfloat16 [2, 4096], replicated, may hold values from 0.099609375 to 1.8984375
- query_weight: bfloat16 [2, 4096, 2048], P(None, None, 'tp'), may hold values from -0.09375 to 0.09375
- key_weight: bfloat16 [2, 4096, 2048], P(None, None, 'tp'), may hold values from -0.09375 to 0.09375
- value_weight: bfloat16 [2, 4096, 8, 256], P(None, None, None, 'tp'), as said below
- gate_weight: bfloat16 [2, 4096, 8, 256], P(None, None, None, 'tp'), may hold values from -0.09375 to 0.09375
- group_gain: bfloat16 [2, 8, 256], P(None, None, 'tp'), may hold values from 0.099609375 to 1.8984375
- output_weight: bfloat16 [2, 8, 256, 4096], P(None, None, 'tp'), may hold values from -0.375 to 0.375
Outputs:
- stream_out: bfloat16 [64, 4, 4096], P('grp', None, 'tp'), parts along dimension 0
- state_out: float32 [2, 64, 8, 256, 256], P(None, 'grp', None, 'tp'), parts along dimension 1
There are 2 independent parts, one for each index of `grp`. A program takes and returns all parts, laid end to end along the dimension named above; an argument that names none is the same for every part. Nothing has to cross between parts.
Inputs may be any that keep to these rules, and one draw needn't show every extreme that they name: `value_weight`: real values; column scales of the value projection differ.
All inputs are finite; a program needn't handle non-finite values.
Results may differ from a plain program's by a relative error of at most 0.024.
Values may be sent and summed in bfloat16 or wider, within the bound.
No kernel may reach another device: no remote copies, remote signals or barrier semaphores. Data moves between devices by JAX's collectives and lax.ppermute only.
A program may use at most 64 MiB of HBM per device.

v0:
```python
import jax
import jax.numpy as jnp
from jax import lax
from jax.sharding import PartitionSpec as P

HEAD_DIM = 256
PAST = 1024
EPS_RMS = 1e-06
EPS_GROUP = 1e-05
ROTARY_BASE = 10000.0


def log_decays(count):
    return jnp.log(1.0 - jnp.power(2.0, -5.0 - jnp.arange(count, dtype=jnp.float32)))


def decay_tables(log_gamma, count):
    steps = jnp.arange(count, dtype=jnp.float32)
    gap = steps[:, None] - steps[None, :]
    intra = jnp.where(
        gap[None] >= 0, jnp.exp(log_gamma[:, None, None] * jnp.maximum(gap, 0.0)[None]), 0.0
    )
    q_decay = jnp.exp(log_gamma[None, :] * (steps[:, None] + 1.0))
    k_decay = jnp.exp(log_gamma[None, :] * (count - 1.0 - steps[:, None]))
    block_decay = jnp.exp(log_gamma * count)
    return (intra, q_decay, k_decay, block_decay)


def rotate(values, offset):
    half_dim = values.shape[-1] // 2
    freqs = jnp.power(
        ROTARY_BASE, -jnp.arange(half_dim, dtype=jnp.float32) * (2.0 / values.shape[-1])
    )
    places = (offset + jnp.arange(values.shape[1])).astype(jnp.float32)
    angles = places[:, None] * freqs[None, :]
    cosine = jnp.cos(angles)[None, :, None, :]
    sine = jnp.sin(angles)[None, :, None, :]
    first = values[..., :half_dim]
    second = values[..., half_dim:]
    return jnp.concatenate(
        [first * cosine - second * sine, second * cosine + first * sine], axis=-1
    )


def local(
    stream_in,
    state_in,
    norm_gain,
    query_weight,
    key_weight,
    value_weight,
    gate_weight,
    group_gain,
    output_weight,
):
    seqs, new_tok, width = stream_in.shape
    heads, local_dim = (value_weight.shape[2], value_weight.shape[3])
    head_dim = HEAD_DIM
    log_gamma = log_decays(heads)
    intra, q_decay, k_decay, block_decay = decay_tables(log_gamma, new_tok)
    highest = lax.Precision.HIGHEST
    share_cols = width // lax.axis_size("tp")
    col_start = lax.axis_index("tp") * share_cols
    layers = state_in.shape[0]
    stream = stream_in
    stream_share = stream_in
    new_states = []
    for layer_no in range(layers):
        stream_f = stream.astype(jnp.float32)
        normed = stream_f * lax.rsqrt(
            jnp.mean(stream_f * stream_f, axis=-1, keepdims=True) + EPS_RMS
        )
        normed = (normed * norm_gain[layer_no].astype(jnp.float32)).astype(jnp.bfloat16)
        flat = normed.reshape(seqs * new_tok, width)
        query_part = jnp.dot(flat, query_weight[layer_no], preferred_element_type=jnp.float32)
        query_part = query_part.astype(jnp.bfloat16).reshape(seqs, new_tok, -1)
        key_part = jnp.dot(flat, key_weight[layer_no], preferred_element_type=jnp.float32)
        key_part = key_part.astype(jnp.bfloat16).reshape(seqs, new_tok, -1)

        def project_local(weight):
            result = jnp.dot(
                flat, weight.reshape(width, heads * local_dim), preferred_element_type=jnp.float32
            )
            result = lax.optimization_barrier(result.astype(jnp.bfloat16))
            return result.astype(jnp.float32).reshape(seqs, new_tok, heads, local_dim)

        values_f = project_local(value_weight[layer_no])
        gates_f = project_local(gate_weight[layer_no])
        queries, key_rows = (
            lax.all_gather(query_part, "tp", axis=2, tiled=True),
            lax.all_gather(key_part, "tp", axis=2, tiled=True),
        )
        queries = queries.astype(jnp.float32).reshape(seqs, new_tok, heads, head_dim)
        key_rows = key_rows.astype(jnp.float32).reshape(seqs, new_tok, heads, head_dim)
        rot_q = rotate(queries, PAST)
        rot_k = rotate(key_rows, PAST) * head_dim ** (-0.5)
        scores = jnp.einsum("bthd,bshd->bhts", rot_q, rot_k, precision=highest) * intra[None]
        inner = jnp.einsum("bhts,bshe->bthe", scores, values_f, precision=highest)
        state = state_in[layer_no]
        carried = (
            jnp.einsum("bthd,bhed->bthe", rot_q, state, precision=highest)
            * q_decay[None, :, :, None]
        )
        mixed = inner + carried
        new_state = state * block_decay[None, :, None, None] + jnp.einsum(
            "bthe,bthd->bhed", values_f, rot_k * k_decay[None, :, :, None], precision=highest
        )
        new_states.append(new_state)
        totals, squares = lax.psum((jnp.sum(mixed, axis=-1), jnp.sum(mixed * mixed, axis=-1)), "tp")
        mean_o = (totals / head_dim)[..., None]
        var_o = (squares / head_dim)[..., None] - mean_o * mean_o
        normal = (
            (mixed - mean_o)
            * lax.rsqrt(var_o + EPS_GROUP)
            * group_gain[layer_no].astype(jnp.float32)[None, None]
        )
        gated = (jax.nn.silu(gates_f) * normal).astype(jnp.bfloat16)
        partial_out = jnp.dot(
            gated.reshape(seqs * new_tok, heads * local_dim),
            output_weight[layer_no].reshape(heads * local_dim, width),
            preferred_element_type=jnp.float32,
        ).reshape(seqs, new_tok, width)
        share_out = lax.psum_scatter(partial_out, "tp", scatter_dimension=2, tiled=True)
        own_cols = lax.dynamic_slice_in_dim(stream, col_start, share_cols, 2)
        stream_share = (own_cols.astype(jnp.float32) + share_out).astype(jnp.bfloat16)
        if layer_no + 1 < layers:
            stream = lax.all_gather(stream_share, "tp", axis=2, tiled=True)
    result = stream_share
    return (result, jnp.stack(new_states))


def solution(mesh):
    in_specs = (
        P("grp", None, None),
        P(None, "grp", None, "tp", None),
        P(),
        P(None, None, "tp"),
        P(None, None, "tp"),
        P(None, None, None, "tp"),
        P(None, None, None, "tp"),
        P(None, None, "tp"),
        P(None, None, "tp", None),
    )
    out_specs = (P("grp", None, "tp"), P(None, "grp", None, "tp", None))
    return jax.shard_map(local, mesh=mesh, in_specs=in_specs, out_specs=out_specs, check_vma=False)
```

profile of v0, /device:TPU:0, one launch (start us, length us, event | category | flops | bytes accessed | tf_op | source)
XLA Modules:
  0.0 433.5 jit_solution(2907268632619906550)
XLA Ops:
  7.3 0.7 bitcast_convert_fusion
  8.0 1.8 fusion.10
  9.9 0.8 slice_convert_fusion
  10.7 1.9 fusion.12
  12.6 0.3 reshape.316
  12.9 1.8 convolution_convert_fusion.4
  14.8 0.4 convolution_convert_fusion.5
  15.2 24.6 %all_gather.15 = bf16[32,4,2048]{2,1,0:T(4,128)(2,1)S(1)} all-gather(bf16[32,4,128]{2,1,0:T(4,128)(2,1)S(1)} %bitcast.115), channel_id=1, replica_groups=mesh['grp'=2,'tp'=16] {'tp'}, dimensions={2}, use_global_device_ids=true | all-gather | bytes 557056 | tf_op jit(solution)/shard_map/all_gather | solution.py:90
  39.8 19.0 %all_gather.16 = bf16[32,4,2048]{2,1,0:T(4,128)(2,1)S(1)} all-gather(bf16[32,4,128]{2,1,0:T(4,128)(2,1)S(1)} %bitcast.114), channel_id=1, replica_groups=mesh['grp'=2,'tp'=16] {'tp'}, dimensions={2}, use_global_device_ids=true | all-gather | bytes 557056 | tf_op jit(solution)/shard_map/all_gather | solution.py:91
  58.9 0.1 convert.11
  59.0 0.1 convert.10
  59.3 0.6 multiply_subtract_fusion.2
  59.9 6.9 %fusion.4 = f32[32,8,4,16]{3,2,1,0:T(4,128)} fusion(f32[2,32,8,16,256]{4,3,2,1,0:T(8,128)} %param.10, f32[32,4,8,128]{3,1,2,0:T(4,128)S(1)} %get-tuple-element.46, f32[32,4,8,128]{3,1,2,0:T(4,128)S(1)} %get-tuple-element.47), kind=kOutput, calls=%fused_computation.7 | convolution fusion | flops 50593792 | bytes 5308416 | tf_op jit(solution)/shard_map/bthd,bhed->bthe/dot_general | solution.py:101
  66.8 2.0 copy.76
  68.9 2.7 fusion.56
  71.5 0.4 convolution_convert_fusion.6
  72.0 0.2 reshape.319
  72.3 2.3 convolution_multiply_fusion.1
  74.6 1.0 fusion.38
  75.6 0.3 copy.75
  75.9 2.7 fusion.55
  78.7 0.4 convolution_convert_fusion.7
  79.1 0.2 reshape.338
  79.3 0.3 copy.73
  79.6 1.8 fusion.54
  81.4 0.2 fusion.51
  81.6 59.1 %all-reduce.1 = (f32[32,4,8]{0,2,1:T(8,128)S(1)}, f32[32,4,8]{0,2,1:T(8,128)S(1)}) all-reduce(f32[32,4,8]{0,2,1:T(8,128)S(1)} %get-tuple-element.15, f32[32,4,8]{0,2,1:T(8,128)S(1)} %get-tuple-element.14), channel_id=1, replica_groups=mesh['grp'=2,'tp'=16] {'tp'}, use_global_device_ids=true, to_apply=%region_4.5 | all-reduce | flops 2048 | bytes 16384 | tf_op jit(solution)/shard_map/psum | solution.py:109
  140.9 1.8 fusion.57
  142.8 0.9 constant_dynamic-slice_fusion
  143.6 58.3 %reduce-scatter.3.cloned.1.call-done = f32[32,4,256]{2,0,1:T(8,128)} async-done(((f32[32,4,4096]{2,0,1:T(8,128)}), f32[32,4,256]{2,0,1:T(8,128)}) %reduce-scatter.3.cloned.1.call-update) | async-done | bytes 131088 | tf_op jit(solution)/shard_map/reduce_scatter | solution.py:123
  201.9 1.5 add_convert_fusion.1
  203.5 0.3 reduce-scatter.5.cloned.1.call-start
  203.8 36.5 %all-gather.2.cloned.1.call-done = bf16[32,4,4096]{2,0,1:T(8,128)(2,1)} async-done(((bf16[32,4,256]{2,0,1:T(8,128)(2,1)}), bf16[32,4,4096]{2,0,1:T(8,128)(2,1)}) %all-gather.2.cloned.1.call-update) | async-done | bytes 1048592 | tf_op jit(solution)/shard_map/all_gather | solution.py:127
  240.3 1.5 fusion.13
  241.8 1.5 fusion.15
  243.4 0.8 copy.78
  244.2 0.3 reshape.326
  244.5 1.7 convolution_convert_fusion
  246.2 1.7 convolution_convert_fusion.1
  248.0 0.4 convolution_convert_fusion.2
  248.4 0.4 convolution_convert_fusion.3
  248.9 0.2 reshape.329
  249.1 21.5 %all_gather.19 = bf16[32,4,2048]{2,1,0:T(4,128)(2,1)S(1)} all-gather(bf16[32,4,128]{2,1,0:T(4,128)(2,1)S(1)} %bitcast.113), channel_id=1, replica_groups=mesh['grp'=2,'tp'=16] {'tp'}, dimensions={2}, use_global_device_ids=true | all-gather | bytes 557056 | tf_op jit(solution)/shard_map/all_gather | solution.py:91
  270.6 18.9 %all_gather.18 = bf16[32,4,2048]{2,1,0:T(4,128)(2,1)S(1)} all-gather(bf16[32,4,128]{2,1,0:T(4,128)(2,1)S(1)} %bitcast.112), channel_id=1, replica_groups=mesh['grp'=2,'tp'=16] {'tp'}, dimensions={2}, use_global_device_ids=true | all-gather | bytes 557056 | tf_op jit(solution)/shard_map/all_gather | solution.py:90
  289.5 0.2 reshape.346
  289.6 1.0 copy.80
  290.7 0.1 convert.12
  290.8 0.1 convert.13
  291.0 0.5 multiply_subtract_fusion
  291.4 0.8 copy-done.8
  292.2 6.6 %fusion = f32[32,8,4,16]{3,2,1,0:T(4,128)} fusion(f32[2,32,8,16,256]{4,3,2,1,0:T(8,128)} %param.10, f32[32,4,8,128]{3,1,2,0:T(4,128)S(1)} %get-tuple-element.44, f32[32,4,8,128]{3,1,2,0:T(4,128)S(1)} %get-tuple-element.45), kind=kOutput, calls=%fused_computation.2 | convolution fusion | flops 50593792 | bytes 5308416 | tf_op jit(solution)/shard_map/bthd,bhed->bthe/dot_general | solution.py:101
  298.8 1.3 copy.83
  300.1 3.4 convolution_multiply_fusion
  303.5 1.0 fusion.35
  304.5 0.3 copy.82
  304.8 0.2 fusion.50
  305.0 59.2 %all-reduce = (f32[32,4,8]{0,2,1:T(8,128)S(1)}, f32[32,4,8]{0,2,1:T(8,128)S(1)}) all-reduce(f32[32,4,8]{0,2,1:T(8,128)S(1)} %get-tuple-element.13, f32[32,4,8]{0,2,1:T(8,128)S(1)} %get-tuple-element.12), channel_id=1, replica_groups=mesh['grp'=2,'tp'=16] {'tp'}, use_global_device_ids=true, to_apply=%region_10.11 | all-reduce | flops 2048 | bytes 16384 | tf_op jit(solution)/shard_map/psum | solution.py:109
  364.4 1.8 fusion.58
  366.3 4.5 %fusion.7 = f32[1,32,8,16,256]{4,3,2,1,0:T(8,128)S(1)} fusion(f32[2,32,8,16,256]{4,3,2,1,0:T(8,128)} %param.10, f32[8]{0:T(128)S(1)} %multiply_exponential_fusion.1, f32[32,4,8,128]{3,1,2,0:T(4,128)S(1)} %copy-done.5, f32[32,4,8,128]{3,1,2,0:T(4,128)S(1)} %copy-done.3, f32[4,8]{0,1:T(8,128)S(1)} %copy.85, bf16[32,4,8,16]{3,2,1,0:T(8,128)(2,1)S(1)} %reshape.319), kind=kOutput, calls=%fused_computation.10 | convolution fusion | flops 52953088 | bytes 9470112 | tf_op jit(solution)/shard_map/bthe,bthd->bhed/dot_general | solution.py:105
  370.8 4.5 %fusion.3 = f32[1,32,8,16,256]{4,3,2,1,0:T(8,128)S(1)} fusion(f32[2,32,8,16,256]{4,3,2,1,0:T(8,128)} %param.10, f32[8]{0:T(128)S(1)} %multiply_exponential_fusion.1, f32[32,4,8,128]{3,1,2,0:T(4,128)S(1)} %copy-done.7, f32[32,4,8,128]{3,1,2,0:T(4,128)S(1)} %get-tuple-element.28, f32[4,8]{0,1:T(8,128)S(1)} %copy.85, bf16[32,4,8,16]{3,2,1,0:T(8,128)(2,1)S(1)} %reshape.329), kind=kOutput, calls=%fused_computation.5 | convolution fusion | flops 52953088 | bytes 9470112 | tf_op jit(solution)/shard_map/bthe,bthd->bhed/dot_general | solution.py:105
  375.3 4.4 %pad_maximum_fusion = f32[2,32,8,16,256]{4,3,2,1,0:T(8,128)} fusion(f32[1,32,8,16,256]{4,3,2,1,0:T(8,128)S(1)} %fusion.3, f32[1,32,8,16,256]{4,3,2,1,0:T(8,128)S(1)} %fusion.7), kind=kLoop, calls=%fused_computation | loop fusion | flops 2097152 | bytes 16777216 | tf_op jit(solution)/shard_map/stack | solution.py:129
  379.8 45.6 %reduce-scatter.5.cloned.1.call-done = f32[32,4,256]{2,0,1:T(8,128)} async-done(((f32[32,4,4096]{2,0,1:T(8,128)}), f32[32,4,256]{2,0,1:T(8,128)}) %reduce-scatter.5.cloned.1.call-update) | async-done | bytes 131088 | tf_op jit(solution)/shard_map/reduce_scatter | solution.py:123
  425.4 0.9 add_convert_fusion
  426.3 0.7 copy.88
  (45 shorter events, 1.0 us)
Async XLA Ops:
  7.2 194.8 %reduce-scatter.3.cloned.1.call-start = ((), (), s32[]{:S(2)}) async-start(), calls=%async_computation.2 | async-start | bytes 2228224 | tf_op jit(solution)/shard_map/reduce_scatter | solution.py:123
  12.9 1.9 copy-start.11
  59.9 12.4 %copy-start.2 = (f32[32,4,8,128]{3,1,2,0:T(4,128)}, f32[32,4,8,128]{3,1,2,0:T(4,128)S(1)}, u32[]{:S(2)}) copy-start(f32[32,4,8,128]{3,1,2,0:T(4,128)S(1)} %get-tuple-element.32) | copy-start | bytes 1572868
  59.9 12.4 %copy-start.4 = (f32[32,4,8,128]{3,1,2,0:T(4,128)}, f32[32,4,8,128]{3,1,2,0:T(4,128)S(1)}, u32[]{:S(2)}) copy-start(f32[32,4,8,128]{3,1,2,0:T(4,128)S(1)} %get-tuple-element.33) | copy-start | bytes 1572868
  79.6 1.9 copy-start.9
  142.7 97.6 %all-gather.2.cloned.1.call-start = ((), (), s32[]{:S(2)}) async-start(), calls=%async_computation.3 | async-start | bytes 1114112 | tf_op jit(solution)/shard_map/all_gather | solution.py:127
  203.5 221.9 %reduce-scatter.5.cloned.1.call-start = ((), (), s32[]{:S(2)}) async-start(), calls=%async_computation.4 | async-start | bytes 2228224 | tf_op jit(solution)/shard_map/reduce_scatter | solution.py:123
  244.5 3.5 copy-start
  246.2 2.2 copy-start.1
  291.4 0.8 copy-start.8
  291.4 8.7 %copy-start.6 = (f32[32,4,8,128]{3,1,2,0:T(4,128)}, f32[32,4,8,128]{3,1,2,0:T(4,128)S(1)}, u32[]{:S(2)}) copy-start(f32[32,4,8,128]{3,1,2,0:T(4,128)S(1)} %get-tuple-element.29) | copy-start | bytes 1572868
  303.5 60.8 %copy-start.10 = (f32[32,4,8,16]{0,3,2,1:T(8,128)S(1)}, f32[32,4,8,16]{0,3,2,1:T(8,128)}, u32[]{:S(2)}) copy-start(f32[32,4,8,16]{0,3,2,1:T(8,128)} %copy.80) | copy-start | bytes 196612
  364.4 2.0 copy-start.3
  364.4 1.9 copy-start.5
  366.3 4.5 %copy-start.7 = (f32[32,4,8,128]{3,1,2,0:T(4,128)S(1)}, f32[32,4,8,128]{3,1,2,0:T(4,128)}, u32[]{:S(2)}) copy-start(f32[32,4,8,128]{3,1,2,0:T(4,128)} %copy-done.6) | copy-start | bytes 1572868
Sparse Core Ops, SparseCore 0:
  142.8 59.0 reduce-scatter.2
  204.7 35.5 all-gather.1
  366.3 58.9 reduce-scatter.4
where the time goes:
time: 434 us
  blocking collectives  202 us (47%)
  waiting for transfers between devices  140 us (32%)
  matrix products  41.1 us (9%)
  other arithmetic  17.9 us (4%)
  local copies, waits for them, and re-layouts  17.2 us (4%)
  between operations  14.2 us (3%)
    psum x2, blocking collectives, local(): lax.psum((jnp.sum(mixed, axis=-1), jnp.sum(mixed * mixed, axis=-1)), 'tp')  118 us
    reduce_scatter x2, waiting for transfers between devices, local(): lax.psum_scatter(partial_out, 'tp', scatter_dimension=2, tiled=True)  104 us
    all_gather x2, blocking collectives, local(): lax.all_gather(query_part, 'tp', axis=2, tiled=True)  43.5 us
    all_gather x2, blocking collectives, local(): lax.all_gather(key_part, 'tp', axis=2, tiled=True)  40.6 us
    all_gather x1, waiting for transfers between devices, local(): stream = lax.all_gather(stream_share, 'tp', axis=2, tiled=True)  36.5 us
    dot_general x2, matrix products, local(): jnp.einsum('bthd,bhed->bthe', rot_q, state, precision=highest)  13.5 us
    dot_general x2, matrix products, local(): jnp.einsum('bthe,bthd->bhed', values_f, rot_k * k_decay[None, :, :, None]...  8.98 us
  transfers between devices with their start and end apart: 3, of which 3 were waited for; matrix products, arithmetic and copies ran while one was open for 3% of the time, Pallas kernels for 0%

commit v1 on v0

--- a/solution.py
+++ b/solution.py
@@ -8,6 +8,11 @@
 EPS_RMS = 1e-06
 EPS_GROUP = 1e-05
 ROTARY_BASE = 10000.0
+
+
+def gather_blocks(shard, mesh_axis, dim):
+    blocks = lax.all_gather(shard, mesh_axis)
+    return jnp.concatenate(blocks, axis=dim)
 
 
 def log_decays(count):
@@ -88,7 +93,7 @@
         gates_f = project_local(gate_weight[layer_no])
         queries, key_rows = (
             lax.all_gather(query_part, "tp", axis=2, tiled=True),
-            lax.all_gather(key_part, "tp", axis=2, tiled=True),
+            gather_blocks(key_part, "tp", 2),
         )
         queries = queries.astype(jnp.float32).reshape(seqs, new_tok, heads, head_dim)
         key_rows = key_rows.astype(jnp.float32).reshape(seqs, new_tok, heads, head_dim)

time: 434 us -> 441 us (1.016)
  local copies, waits for them, and re-layouts: 17.2 us -> 22.3 us
where the time goes in v1:
time: 441 us; the launch traced here: 440 us
  blocking collectives  204 us (46%)
  waiting for transfers between devices  141 us (32%)
  matrix products  40.6 us (9%)
  local copies, waits for them, and re-layouts  22.3 us (5%)
  other arithmetic  18.6 us (4%)
  between operations  14.2 us (3%)
    psum x2, blocking collectives, local(): lax.psum((jnp.sum(mixed, axis=-1), jnp.sum(mixed * mixed, axis=-1)), 'tp')  118 us
    reduce_scatter x2, waiting for transfers between devices, local(): lax.psum_scatter(partial_out, 'tp', scatter_dimension=2, tiled=True)  104 us
    all_gather x2, blocking collectives, local(): lax.all_gather(query_part, 'tp', axis=2, tiled=True)  44.9 us
    all_gather x2, blocking collectives, gather_blocks(): blocks = lax.all_gather(shard, mesh_axis)  40.5 us
    all_gather x1, waiting for transfers between devices, local(): stream = lax.all_gather(stream_share, 'tp', axis=2, tiled=True)  36.7 us
    dot_general x2, matrix products, local(): jnp.einsum('bthd,bhed->bthe', rot_q, state, precision=highest)  12.8 us
    dot_general x2, matrix products, local(): jnp.einsum('bthe,bthd->bhed', values_f, rot_k * k_decay[None, :, :, None]...  8.98 us
  transfers between devices with their start and end apart: 3, of which 3 were waited for; matrix products, arithmetic and copies ran while one was open for 3% of the time, Pallas kernels for 0%

profile of v1, /device:TPU:0, one launch (start us, length us, event | category | flops | bytes accessed | tf_op | source)
XLA Modules:
  0.0 440.4 jit_solution(16511078269712216681)
XLA Ops:
  7.3 0.7 bitcast_convert_fusion
  8.0 1.8 fusion.10
  9.9 0.8 slice_convert_fusion
  10.7 1.9 fusion.12
  12.6 0.3 reshape.310
  12.9 1.8 convolution_convert_fusion.4
  14.8 0.4 convolution_convert_fusion.5
  15.2 26.1 %all_gather.15 = bf16[32,4,2048]{2,1,0:T(4,128)(2,1)} all-gather(bf16[32,4,128]{2,1,0:T(4,128)(2,1)S(1)} %bitcast.115), channel_id=1, replica_groups=mesh['grp'=2,'tp'=16] {'tp'}, dimensions={2}, use_global_device_ids=true | all-gather | bytes 557056 | tf_op jit(solution)/shard_map/all_gather | solution.py:95
  41.3 19.0 %all_gather.16 = bf16[16,32,4,128]{3,1,2,0:T(8,128)(2,1)S(1)} all-gather(bf16[1,32,4,128]{3,1,2,0:T(8,128)(2,1)S(1)} %copy.96), channel_id=1, replica_groups=mesh['grp'=2,'tp'=16] {'tp'}, dimensions={0}, use_global_device_ids=true | all-gather | bytes 557056 | tf_op jit(solution)/shard_map/all_gather | solution.py:14
  60.4 0.6 copy.97
  61.1 0.3 reshape.329
  61.5 0.9 copy-done.9
  62.7 0.6 multiply_subtract_fusion.2
  63.3 6.9 %fusion.4 = f32[32,8,4,16]{3,2,1,0:T(4,128)} fusion(f32[2,32,8,16,256]{4,3,2,1,0:T(8,128)} %param.10, f32[32,4,8,128]{3,1,2,0:T(4,128)S(1)} %get-tuple-element.50, f32[32,4,8,128]{3,1,2,0:T(4,128)S(1)} %get-tuple-element.51), kind=kOutput, calls=%fused_computation.7 | convolution fusion | flops 50593792 | bytes 5308416 | tf_op jit(solution)/shard_map/bthd,bhed->bthe/dot_general | solution.py:106
  70.3 2.0 copy.102
  72.3 2.7 fusion.56
  75.0 0.4 convolution_convert_fusion.6
  75.4 0.2 reshape.313
  75.7 2.3 convolution_multiply_fusion.1
  78.0 1.0 fusion.38
  79.0 0.3 copy.101
  79.3 2.7 fusion.55
  82.0 0.4 convolution_convert_fusion.7
  82.7 0.3 copy.95
  83.0 1.8 fusion.54
  84.8 0.2 fusion.51
  85.0 59.1 %all-reduce.1 = (f32[32,4,8]{0,2,1:T(8,128)S(1)}, f32[32,4,8]{0,2,1:T(8,128)S(1)}) all-reduce(f32[32,4,8]{0,2,1:T(8,128)S(1)} %get-tuple-element.15, f32[32,4,8]{0,2,1:T(8,128)S(1)} %get-tuple-element.14), channel_id=1, replica_groups=mesh['grp'=2,'tp'=16] {'tp'}, use_global_device_ids=true, to_apply=%region_4.5 | all-reduce | flops 2048 | bytes 16384 | tf_op jit(solution)/shard_map/psum | solution.py:114
  144.3 1.8 fusion.59
  146.1 0.3 all-gather.2.cloned.1.call-start
  146.4 0.9 constant_dynamic-slice_fusion
  147.3 58.1 %reduce-scatter.3.cloned.1.call-done = f32[32,4,256]{2,0,1:T(8,128)} async-done(((f32[32,4,4096]{2,0,1:T(8,128)}), f32[32,4,256]{2,0,1:T(8,128)}) %reduce-scatter.3.cloned.1.call-update) | async-done | bytes 131088 | tf_op jit(solution)/shard_map/reduce_scatter | solution.py:128
  205.3 1.5 add_convert_fusion.1
  207.0 36.7 %all-gather.2.cloned.1.call-done = bf16[32,4,4096]{2,0,1:T(8,128)(2,1)} async-done(((bf16[32,4,256]{2,0,1:T(8,128)(2,1)}), bf16[32,4,4096]{2,0,1:T(8,128)(2,1)}) %all-gather.2.cloned.1.call-update) | async-done | bytes 1048592 | tf_op jit(solution)/shard_map/all_gather | solution.py:132
  243.7 1.5 fusion.13
  245.2 1.5 fusion.15
  246.8 0.8 copy.104
  247.6 0.3 reshape.317
  247.9 1.7 convolution_convert_fusion
  249.6 1.7 convolution_convert_fusion.1
  251.4 0.4 convolution_convert_fusion.2
  251.9 0.4 convolution_convert_fusion.3
  252.3 0.9 reshape.320
  253.2 21.5 %all_gather.19 = bf16[16,32,4,128]{3,1,2,0:T(8,128)(2,1)S(1)} all-gather(bf16[1,32,4,128]{3,1,2,0:T(8,128)(2,1)S(1)} %copy.107), channel_id=1, replica_groups=mesh['grp'=2,'tp'=16] {'tp'}, dimensions={0}, use_global_device_ids=true | all-gather | bytes 557056 | tf_op jit(solution)/shard_map/all_gather | solution.py:14
  274.7 18.9 %all_gather.18 = bf16[32,4,2048]{2,1,0:T(4,128)(2,1)S(1)} all-gather(bf16[32,4,128]{2,1,0:T(4,128)(2,1)S(1)} %bitcast.114), channel_id=1, replica_groups=mesh['grp'=2,'tp'=16] {'tp'}, dimensions={2}, use_global_device_ids=true | all-gather | bytes 557056 | tf_op jit(solution)/shard_map/all_gather | solution.py:95
  293.8 1.0 copy.106
  295.1 1.6 copy.108
  296.7 1.5 reshape.336
  298.3 1.3 multiply_subtract_fusion
  299.6 0.8 copy-done.10
  300.4 0.2 copy-done.11
  300.6 5.8 %fusion = f32[32,8,4,16]{3,2,1,0:T(4,128)S(1)} fusion(f32[2,32,8,16,256]{4,3,2,1,0:T(8,128)} %param.10, f32[32,4,8,128]{3,1,2,0:T(4,128)S(1)} %get-tuple-element.48, f32[32,4,8,128]{3,1,2,0:T(4,128)S(1)} %get-tuple-element.49), kind=kOutput, calls=%fused_computation.2 | convolution fusion | flops 50593792 | bytes 5308416 | tf_op jit(solution)/shard_map/bthd,bhed->bthe/dot_general | solution.py:106
  306.4 0.3 copy.113
  306.8 3.6 convolution_multiply_fusion
  310.3 1.0 fusion.35
  311.3 0.3 copy.112
  311.7 0.2 fusion.50
  311.8 59.2 %all-reduce = (f32[32,4,8]{0,2,1:T(8,128)S(1)}, f32[32,4,8]{0,2,1:T(8,128)S(1)}) all-reduce(f32[32,4,8]{0,2,1:T(8,128)S(1)} %get-tuple-element.13, f32[32,4,8]{0,2,1:T(8,128)S(1)} %get-tuple-element.12), channel_id=1, replica_groups=mesh['grp'=2,'tp'=16] {'tp'}, use_global_device_ids=true, to_apply=%region_10.11 | all-reduce | flops 2048 | bytes 16384 | tf_op jit(solution)/shard_map/psum | solution.py:114
  371.2 1.8 fusion.60
  373.2 4.5 %fusion.7 = f32[1,32,8,16,256]{4,3,2,1,0:T(8,128)S(1)} fusion(f32[2,32,8,16,256]{4,3,2,1,0:T(8,128)} %param.10, f32[8]{0:T(128)S(1)} %multiply_exponential_fusion.1, f32[32,4,8,128]{3,1,2,0:T(4,128)S(1)} %copy-done.6, f32[32,4,8,128]{3,1,2,0:T(4,128)S(1)} %copy-done.4, f32[4,8]{0,1:T(8,128)S(1)} %copy.115, bf16[32,4,8,16]{3,2,1,0:T(8,128)(2,1)S(1)} %reshape.313), kind=kOutput, calls=%fused_computation.10 | convolution fusion | flops 52953088 | bytes 9470112 | tf_op jit(solution)/shard_map/bthe,bthd->bhed/dot_general | solution.py:110
  377.7 4.5 %fusion.3 = f32[1,32,8,16,256]{4,3,2,1,0:T(8,128)S(1)} fusion(f32[2,32,8,16,256]{4,3,2,1,0:T(8,128)} %param.10, f32[8]{0:T(128)S(1)} %multiply_exponential_fusion.1, f32[32,4,8,128]{3,1,2,0:T(4,128)S(1)} %copy-done.8, f32[32,4,8,128]{3,1,2,0:T(4,128)S(1)} %get-tuple-element.28, f32[4,8]{0,1:T(8,128)S(1)} %copy.115, bf16[32,4,8,16]{3,2,1,0:T(8,128)(2,1)S(1)} %copy-done.2), kind=kOutput, calls=%fused_computation.5 | convolution fusion | flops 52953088 | bytes 9470112 | tf_op jit(solution)/shard_map/bthe,bthd->bhed/dot_general | solution.py:110
  382.2 4.4 %pad_maximum_fusion = f32[2,32,8,16,256]{4,3,2,1,0:T(8,128)} fusion(f32[1,32,8,16,256]{4,3,2,1,0:T(8,128)S(1)} %fusion.3, f32[1,32,8,16,256]{4,3,2,1,0:T(8,128)S(1)} %fusion.7), kind=kLoop, calls=%fused_computation | loop fusion | flops 2097152 | bytes 16777216 | tf_op jit(solution)/shard_map/stack | solution.py:134
  386.6 45.6 %reduce-scatter.5.cloned.1.call-done = f32[32,4,256]{2,0,1:T(8,128)} async-done(((f32[32,4,4096]{2,0,1:T(8,128)}), f32[32,4,256]{2,0,1:T(8,128)}) %reduce-scatter.5.cloned.1.call-update) | async-done | bytes 131088 | tf_op jit(solution)/shard_map/reduce_scatter | solution.py:128
  432.2 0.9 add_convert_fusion
  433.2 0.7 copy.118
  (59 shorter events, 2.1 us)
Async XLA Ops:
  7.2 198.2 %reduce-scatter.3.cloned.1.call-start = ((), (), s32[]{:S(2)}) async-start(), calls=%async_computation.2 | async-start | bytes 2228224 | tf_op jit(solution)/shard_map/reduce_scatter | solution.py:128
  12.9 1.9 copy-start.14
  61.4 1.0 copy-start.9
  63.3 12.4 %copy-start.3 = (f32[32,4,8,128]{3,1,2,0:T(4,128)}, f32[32,4,8,128]{3,1,2,0:T(4,128)S(1)}, u32[]{:S(2)}) copy-start(f32[32,4,8,128]{3,1,2,0:T(4,128)S(1)} %get-tuple-element.32) | copy-start | bytes 1572868
  63.3 12.4 %copy-start.5 = (f32[32,4,8,128]{3,1,2,0:T(4,128)}, f32[32,4,8,128]{3,1,2,0:T(4,128)S(1)}, u32[]{:S(2)}) copy-start(f32[32,4,8,128]{3,1,2,0:T(4,128)S(1)} %get-tuple-element.33) | copy-start | bytes 1572868
  83.0 1.9 copy-start.12
  146.1 97.6 %all-gather.2.cloned.1.call-start = ((), (), s32[]{:S(2)}) async-start(), calls=%async_computation.3 | async-start | bytes 1114112 | tf_op jit(solution)/shard_map/all_gather | solution.py:132
  206.9 225.3 %reduce-scatter.5.cloned.1.call-start = ((), (), s32[]{:S(2)}) async-start(), calls=%async_computation.4 | async-start | bytes 2228224 | tf_op jit(solution)/shard_map/reduce_scatter | solution.py:128
  247.9 3.5 copy-start
  249.6 2.2 copy-start.1
  299.6 0.8 copy-start.10
  299.6 1.0 copy-start.11
  300.6 6.2 %copy-start.7 = (f32[32,4,8,128]{3,1,2,0:T(4,128)S(1)}, f32[32,4,8,128]{3,1,2,0:T(4,128)}, u32[]{:S(2)}) copy-start(f32[32,4,8,128]{3,1,2,0:T(4,128)} %get-tuple-element.29) | copy-start | bytes 1572868
  306.8 3.6 copy-start.2
  310.3 60.8 %copy-start.13 = (f32[32,4,8,16]{0,3,2,1:T(8,128)S(1)}, f32[32,4,8,16]{0,3,2,1:T(8,128)}, u32[]{:S(2)}) copy-start(f32[32,4,8,16]{0,3,2,1:T(8,128)} %copy.106) | copy-start | bytes 196612
  371.2 1.9 copy-start.4
  371.2 1.9 copy-start.6
  373.2 4.5 %copy-start.8 = (f32[32,4,8,128]{3,1,2,0:T(4,128)S(1)}, f32[32,4,8,128]{3,1,2,0:T(4,128)}, u32[]{:S(2)}) copy-start(f32[32,4,8,128]{3,1,2,0:T(4,128)} %get-tuple-element.29) | copy-start | bytes 1572868
Sparse Core Ops, SparseCore 0:
  146.2 59.0 reduce-scatter.2
  208.1 35.5 all-gather.1
  373.2 59.0 reduce-scatter.4
